TPU v7x, 32 devices: a whole 2x2x4 slice. The times are simulated.
32 devices in a mesh: sp: 8 (over z, y), tp: 4 (over x, core).
Axes of the slice: x: 2, y: 2, z: 4, core: 2. Of those that a mesh axis runs over, the one named last changes fastest.
Arguments:
- proj_value: bfloat16 [4096, 2016], P('sp', 'tp'), may hold values from -6 to 6
- proj_gate: bfloat16 [4096, 2016], P('sp', 'tp'), may hold values from -8 to 8
- conv_saved: bfloat16 [4096, 2016], P('sp', 'tp'), may hold values from -12 to 12
- conv_taps: bfloat16 [31, 2016], P(None, 'tp'), may hold values from -1 to 1
- norm_gain: bfloat16 [2016], P('tp'), may hold values from 0.099609375 to 1.8984375
- out_weight: bfloat16 [2016, 2016], P('tp'), may hold values from -0.125 to 0.125
- cotangent: bfloat16 [4096, 2016], P('sp'), may hold values from -6 to 6
Outputs:
- grad_value: bfloat16 [4096, 2016], P('sp', 'tp')
- grad_gate: bfloat16 [4096, 2016], P('sp', 'tp')
- grad_out_weight: float32 [2016, 2016], P('tp', 'sp')
- grad_taps: float32 [31, 2016], P(None, 'tp')
All inputs are finite; a program needn't handle non-finite values.
Results may differ from a plain program's by a relative error of at most 0.003.
Values sent between devices are 32-bit elements; how exact they have to be, the bound alone decides.
A program may use at most 64 MiB of HBM per device.

v0:
```python
import math
import jax
import jax.numpy as jnp
from jax import lax
from jax.sharding import PartitionSpec as P

norm_eps = 1e-05


def passed_along(block, axis, distance):
    devices = range(lax.axis_size(axis))
    route = [(i - distance, i) for i in devices if i - distance in devices]
    return lax.ppermute(block, axis, route)


def local(proj_value, proj_gate, conv_saved, conv_taps, norm_gain, out_weight, cotangent):
    model_width = cotangent.shape[1]
    tok_rows = cotangent.shape[0]
    tap_count = conv_taps.shape[0]
    overhang = tap_count - 1
    grad_scale = 1.0 / math.sqrt(tok_rows * lax.axis_size("sp"))
    conv_f = conv_saved.astype(jnp.float32)
    totals = lax.psum((jnp.sum(conv_f, axis=1), jnp.sum(conv_f * conv_f, axis=1)), "tp")
    row_mean = totals[0] / model_width
    row_var = totals[1] / model_width - row_mean * row_mean
    inv_std = lax.rsqrt(row_var + norm_eps)
    centered = (conv_f - row_mean[:, None]) * inv_std[:, None]
    gain_f = norm_gain.astype(jnp.float32)
    normed = centered * gain_f
    gate_norm = jax.nn.sigmoid(normed)
    activated = (normed * gate_norm).astype(jnp.bfloat16)
    contract_rows = (((0,), (0,)), ((), ()))
    whole_term = lax.dot_general(
        cotangent, activated, contract_rows, preferred_element_type=jnp.float32
    )
    shard_grad = lax.psum_scatter(whole_term, "sp", scatter_dimension=0, tiled=True)
    grad_out_weight = shard_grad.T * grad_scale
    d_act = lax.dot_general(
        cotangent, out_weight, (((1,), (1,)), ((), ())), preferred_element_type=jnp.float32
    )
    d_hat = d_act * gate_norm * (1.0 + normed * (1.0 - gate_norm)) * gain_f
    moments = lax.psum((jnp.sum(d_hat, axis=1), jnp.sum(d_hat * centered, axis=1)), "tp")
    first = moments[0] / model_width
    second = moments[1] / model_width
    d_conv = inv_std[:, None] * (d_hat - first[:, None] - centered * second[:, None])
    ahead = passed_along(d_conv[:overhang], "sp", -1)
    extended = jnp.concatenate([d_conv, ahead], axis=0)
    gate_proj = jax.nn.sigmoid(proj_gate.astype(jnp.float32))
    gated = proj_value.astype(jnp.float32) * gate_proj
    taps_f = conv_taps.astype(jnp.float32)
    d_glu = jnp.zeros_like(d_conv)
    tap_rows = []
    for offset in range(tap_count):
        shifted = extended[overhang - offset : overhang - offset + tok_rows]
        d_glu = d_glu + taps_f[offset] * shifted
        tap_rows.append(jnp.sum(gated * shifted, axis=0))
    grad_taps = lax.psum(jnp.stack(tap_rows), "sp") * grad_scale
    grad_value = (d_glu * gate_proj).astype(jnp.bfloat16)
    grad_gate = (d_glu * gated * (1.0 - gate_proj)).astype(jnp.bfloat16)
    return (grad_value, grad_gate, grad_out_weight, grad_taps)


def solution(mesh):
    in_specs = (
        P("sp", "tp"),
        P("sp", "tp"),
        P("sp", "tp"),
        P(None, "tp"),
        P("tp"),
        P("tp", None),
        P("sp", None),
    )
    out_specs = (P("sp", "tp"), P("sp", "tp"), P("tp", "sp"), P(None, "tp"))
    return jax.shard_map(local, mesh=mesh, in_specs=in_specs, out_specs=out_specs, check_vma=False)
```

profile of v0, /device:TPU:0, one launch (start us, length us, event | category | flops | bytes accessed | tf_op | source)
XLA Modules:
  0.0 201.0 jit_solution(5492101719931383703)
XLA Ops:
  7.2 0.0 copy-start
  7.2 0.0 all-reduce.5.cloned.1.call-start
  7.2 1.3 fusion.2
  8.6 0.7 convert_element_type.26
  9.3 8.3 %all-reduce.2 = (f32[512]{0:T(512)S(1)}, f32[512]{0:T(512)S(1)}) all-reduce(f32[512]{0:T(512)S(1)} %get-tuple-element.38, f32[512]{0:T(512)S(1)} %get-tuple-element.37), channel_id=1, replica_groups=mesh['sp'=8,'tp'=4] {'tp'}, use_global_device_ids=true, to_apply=%region_3.0 | all-reduce | flops 1024 | bytes 8192 | tf_op jit(solution)/shard_map/psum | solution.py:23
  17.6 0.0 copy-done
  17.6 4.3 %fusion.54 = (f32[512]{0:T(512)S(1)}, f32[512]{0:T(512)S(1)}, f32[512,504]{0,1:T(8,128)}) fusion(f32[512]{0:T(512)S(1)} %get-tuple-element.77, f32[512]{0:T(512)S(1)} %get-tuple-element.78, bf16[512,504]{0,1:T(8,128)(2,1)} %param.9, f32[504]{0:T(512)S(1)} %convert_element_type.26, bf16[512,2016]{0,1:T(8,128)(2,1)S(1)} %copy-done, bf16[504,2016]{1,0:T(8,128)(2,1)} %param.12), kind=kOutput, calls=%fused_computation.159 | convolution fusion | flops 1044577280 | bytes 5655008 | tf_op jit(solution)/shard_map/dot_general | solution.py:38
  21.9 5.7 %all-reduce.1 = (f32[512]{0:T(512)S(1)}, f32[512]{0:T(512)S(1)}) all-reduce(f32[512]{0:T(512)S(1)} %get-tuple-element.36, f32[512]{0:T(512)S(1)} %get-tuple-element.35), channel_id=1, replica_groups=mesh['sp'=8,'tp'=4] {'tp'}, use_global_device_ids=true, to_apply=%region_7.0 | all-reduce | flops 1024 | bytes 8192 | tf_op jit(solution)/shard_map/psum | solution.py:42
  27.6 0.0 copy-start.3
  27.6 1.7 fusion.17
  29.3 0.7 slice.249
  30.0 1.5 collective-permute-start
  31.5 0.0 copy-done.3
  31.5 3.4 %convolution_bitcast_fusion = f32[2016,504]{0,1:T(8,128)} fusion(bf16[512,2016]{0,1:T(8,128)(2,1)S(1)} %copy-done, bf16[512,504]{0,1:T(8,128)(2,1)S(1)} %copy-done.3, f32[504]{0:T(512)S(1)} %convert_element_type.26, f32[512]{0:T(512)S(1)} %get-tuple-element.78, f32[512]{0:T(512)S(1)} %get-tuple-element.77), kind=kOutput, calls=%fused_computation.29 | convolution fusion | flops 1042771968 | bytes 6650848 | tf_op jit(solution)/shard_map/dot_general | solution.py:33
  34.9 0.0 copy-start.4
  34.9 0.0 copy-start.5
  35.0 0.0 all-reduce.5.cloned.1.call-update
  35.0 0.7 copy-done.4
  35.8 0.0 copy-done.5
  35.8 0.6 dynamic-slice
  37.0 3.0 %collective-permute-done = f32[30,504]{0,1:T(8,128)S(1)} collective-permute-done((f32[30,504]{0,1:T(8,128)}, f32[30,504]{0,1:T(8,128)S(1)}, u32[]{:S(2)}, u32[]{:S(2)}) %collective-permute-start) | collective-permute-done | bytes 60512 | tf_op jit(solution)/shard_map/ppermute | solution.py:13
  40.0 0.0 copy-start.1
  40.0 0.0 copy-start.2
  40.0 17.6 %multiply_convert_fusion = (bf16[512,504]{0,1:T(8,128)(2,1)}, f32[512,504]{0,1:T(8,128)S(1)}) fusion(bf16[512,504]{0,1:T(8,128)(2,1)} %param.8, bf16[512,504]{0,1:T(8,128)(2,1)} %param.7, f32[512,504]{0,1:T(8,128)S(1)} %fusion.17, f32[504]{0:T(512)S(1)} %bitcast.109, f32[30,504]{0,1:T(8,128)S(1)} %collective-permute-done, f32[504]{0:T(512)S(1)} %bitcast.108, ...), kind=kLoop, calls=%fused_computation.142 | loop fusion | flops 26062848 | bytes 3735648 | tf_op jit(solution)/shard_map/convert_element_type | solution.py:59
  57.6 0.0 copy-done.1
  57.6 0.0 copy-done.2
  57.7 4.1 %multiply_reduce_fusion.4 = (f32[504]{0:T(512)S(1)}, f32[504]{0:T(512)S(1)}, f32[504]{0:T(512)S(1)}, f32[504]{0:T(512)S(1)}, f32[504]{0:T(512)S(1)}, /*index=5*/...) fusion(f32[30,504]{0,1:T(8,128)S(1)} %collective-permute-done, f32[512,504]{0,1:T(8,128)S(1)} %fusion.17, ...), kind=kLoop, calls=%fused_computation.115 | loop fusion | flops 7221816 | bytes 3687264 | tf_op jit(solution)/shard_map/reduce_sum | solution.py:56
  61.7 4.3 %multiply_reduce_fusion.1 = (f32[504]{0:T(512)S(1)}, f32[504]{0:T(512)S(1)}, f32[504]{0:T(512)S(1)}, f32[504]{0:T(512)S(1)}, f32[504]{0:T(512)S(1)}, /*index=5*/f32[504]{0:T(512)S(1)}, f32[504]{0:T(512)S(1)}, f32[504]{0:T(512)S(1)}) fusion(f32[30,504]{0,1:T(8,128)S(1)} %collective-permute-done, f32[512,504]{0,1:T(8,128)S(1)} %fusion.17, ...), kind=kLoop, calls=%fused_computation.112 | loop fusion | flops 7737408 | bytes 2140992 | tf_op jit(solution)/shard_map/reduce_sum | solution.py:56
  66.1 4.4 %multiply_reduce_fusion.2 = (f32[504]{0:T(512)S(1)}, f32[504]{0:T(512)S(1)}, f32[504]{0:T(512)S(1)}, f32[504]{0:T(512)S(1)}, f32[504]{0:T(512)S(1)}, /*index=5*/f32[504]{0:T(512)S(1)}, f32[504]{0:T(512)S(1)}, f32[504]{0:T(512)S(1)}) fusion(f32[30,504]{0,1:T(8,128)S(1)} %collective-permute-done, f32[512,504]{0,1:T(8,128)S(1)} %fusion.17, ...), kind=kLoop, calls=%fused_computation.113 | loop fusion | flops 7737408 | bytes 2140992 | tf_op jit(solution)/shard_map/reduce_sum | solution.py:56
  70.5 4.4 %multiply_reduce_fusion.3 = (f32[504]{0:T(512)S(1)}, f32[504]{0:T(512)S(1)}, f32[504]{0:T(512)S(1)}, f32[504]{0:T(512)S(1)}, f32[504]{0:T(512)S(1)}, /*index=5*/f32[504]{0:T(512)S(1)}, f32[504]{0:T(512)S(1)}, f32[504]{0:T(512)S(1)}) fusion(f32[30,504]{0,1:T(8,128)S(1)} %collective-permute-done, f32[512,504]{0,1:T(8,128)S(1)} %fusion.17, ...), kind=kLoop, calls=%fused_computation.114 | loop fusion | flops 7737408 | bytes 2140992 | tf_op jit(solution)/shard_map/reduce_sum | solution.py:56
  74.8 0.1 stack.127
  75.0 37.4 %psum.39 = f32[31,504]{1,0:T(8,128)S(1)} all-reduce(f32[31,504]{1,0:T(8,128)S(1)} %stack.127), channel_id=1, replica_groups=mesh['sp'=8,'tp'=4] {'sp'}, use_global_device_ids=true, to_apply=%region_40.0 | all-reduce | flops 15624 | bytes 124992 | tf_op jit(solution)/shard_map/psum | solution.py:57
  112.4 0.6 broadcast_multiply_fusion
  113.1 79.0 %all-reduce.5.cloned.1.call-done = f32[2016,504]{0,1:T(8,128)} async-done(((f32[2016,504]{0,1:T(8,128)}), f32[2016,504]{0,1:T(8,128)}) %all-reduce.5.cloned.1.call-update) | async-done | bytes 4064272
  192.1 2.1 %fusion.48 = f32[504,252]{1,0:T(8,128)} fusion(f32[2016,504]{0,1:T(8,128)} %all-reduce.5.cloned.1.call-done, u32[]{:T(128)S(6)} %multiply.5), kind=kLoop, calls=%fused_computation.148 | loop fusion | flops 127008 | bytes 1016068 | tf_op jit(solution)/shard_map/mul | solution.py:37
  (4 shorter events, 0.1 us)
Async XLA Ops:
  7.2 10.4 %copy-start = (bf16[512,2016]{0,1:T(8,128)(2,1)S(1)}, bf16[512,2016]{0,1:T(8,128)(2,1)}, u32[]{:S(2)}) copy-start(bf16[512,2016]{0,1:T(8,128)(2,1)} %param.13) | copy-start | bytes 6193156
  7.2 184.9 %all-reduce.5.cloned.1.call-start = ((), (), s32[]{:S(2)}) async-start(), calls=%async_computation | async-start | bytes 8257536
  27.6 3.9 %copy-start.3 = (bf16[512,504]{0,1:T(8,128)(2,1)S(1)}, bf16[512,504]{0,1:T(8,128)(2,1)}, u32[]{:S(2)}) copy-start(bf16[512,504]{0,1:T(8,128)(2,1)} %param.9) | copy-start | bytes 1548292
  30.0 10.0 %collective-permute-start = (f32[30,504]{0,1:T(8,128)}, f32[30,504]{0,1:T(8,128)S(1)}, u32[]{:S(2)}, u32[]{:S(2)}) collective-permute-start(f32[30,504]{0,1:T(8,128)} %slice.249), channel_id=1, source_target_pairs={{4,0},{8,4},{12,8},{16,12},{20,16},{24,20},{28,24},{5,1},{9,5},{13... | collective-permute-start | bytes 181448 | tf_op jit(solution)/shard_map/ppermute | solution.py:13
  34.9 0.8 copy-start.4
  34.9 0.8 copy-start.5
  40.0 17.6 %copy-start.1 = (bf16[512,504]{0,1:T(8,128)(2,1)S(1)}, bf16[512,504]{0,1:T(8,128)(2,1)}, u32[]{:S(2)}) copy-start(bf16[512,504]{0,1:T(8,128)(2,1)} %param.8) | copy-start | bytes 1548292
  40.0 17.6 %copy-start.2 = (bf16[512,504]{0,1:T(8,128)(2,1)S(1)}, bf16[512,504]{0,1:T(8,128)(2,1)}, u32[]{:S(2)}) copy-start(bf16[512,504]{0,1:T(8,128)(2,1)} %param.7) | copy-start | bytes 1548292
Sparse Core Ops, SparseCore 0:
  35.1 156.9 all-reduce.4
where the time goes:
time: 201 us
  waiting for transfers between devices  82 us (41%)
  blocking collectives  51.5 us (26%)
  other arithmetic  41.3 us (21%)
  between operations  14.8 us (7%)
  matrix products  7.71 us (4%)
  local copies, waits for them, and re-layouts  2.27 us (1%)
    unnamed x2, waiting for transfers between devices  79 us
    psum x1, blocking collectives, local(): grad_taps = lax.psum(jnp.stack(tap_rows), 'sp') * grad_scale  37.4 us
    convert_element_type x1, other arithmetic, local(): grad_gate = (d_glu * gated * (1.0 - gate_proj)).astype(jnp.bfloat16)  17.6 us
    reduce_sum x4, other arithmetic, local(): tap_rows.append(jnp.sum(gated * shifted, axis=0))  17.2 us
    psum x1, blocking collectives, local(): lax.psum((jnp.sum(conv_f, axis=1), jnp.sum(conv_f * conv_f, axis=1)), 'tp')  8.34 us
    psum x1, blocking collectives, local(): lax.psum((jnp.sum(d_hat, axis=1), jnp.sum(d_hat * centered, axis=1)), 'tp')  5.73 us
    dot_general x1, matrix products, local(): lax.dot_general(cotangent, out_weight, (((1,), (1,)), ((), ())), preferre...  4.27 us
  transfers between devices with their start and end apart: 2, of which 2 were waited for; matrix products, arithmetic and copies ran while one was open for 20% of the time, Pallas kernels for 0%

commit v1 on v0

--- a/solution.py
+++ b/solution.py
@@ -54,7 +54,7 @@
         shifted = extended[overhang - offset : overhang - offset + tok_rows]
         d_glu = d_glu + taps_f[offset] * shifted
         tap_rows.append(jnp.sum(gated * shifted, axis=0))
-    grad_taps = lax.psum(jnp.stack(tap_rows), "sp") * grad_scale
+    grad_taps = jnp.sum(lax.all_gather(jnp.stack(tap_rows), "sp"), axis=0) * grad_scale
     grad_value = (d_glu * gate_proj).astype(jnp.bfloat16)
     grad_gate = (d_glu * gated * (1.0 - gate_proj)).astype(jnp.bfloat16)
     return (grad_value, grad_gate, grad_out_weight, grad_taps)

time: 201 us -> 204 us (1.015)
  waiting for transfers between devices: 82 us -> 88.6 us
  blocking collectives: 51.5 us -> 47.7 us
    psum x1 -> x0, blocking collectives: 37.4 us -> none  [local(): grad_taps = lax.psum(jnp.stack(tap_rows), 'sp') * grad_scale]
    all_gather x0 -> x1, blocking collectives: none -> 33.6 us  [local(): lax.all_gather(jnp.stack(tap_rows), 'sp')]
    unnamed x2, waiting for transfers between devices: 79 us -> 85.6 us
  transfers between devices with their start and end apart: 2 -> 2, of which waited for: 2 -> 2; matrix products, arithmetic and copies ran while one was open for 20% -> 19% of each run, Pallas kernels for 0% -> 0%
where the time goes in v1:
time: 204 us
  waiting for transfers between devices  88.6 us (43%)
  blocking collectives  47.7 us (23%)
  other arithmetic  41.3 us (20%)
  between operations  14.8 us (7%)
  matrix products  7.71 us (4%)
  local copies, waits for them, and re-layouts  2.27 us (1%)
    unnamed x2, waiting for transfers between devices  85.6 us
    all_gather x1, blocking collectives, local(): lax.all_gather(jnp.stack(tap_rows), 'sp')  33.6 us
    convert_element_type x1, other arithmetic, local(): grad_gate = (d_glu * gated * (1.0 - gate_proj)).astype(jnp.bfloat16)  17.6 us
    reduce_sum x4, other arithmetic, local(): tap_rows.append(jnp.sum(gated * shifted, axis=0))  17.1 us
    psum x1, blocking collectives, local(): lax.psum((jnp.sum(conv_f, axis=1), jnp.sum(conv_f * conv_f, axis=1)), 'tp')  8.34 us
    psum x1, blocking collectives, local(): lax.psum((jnp.sum(d_hat, axis=1), jnp.sum(d_hat * centered, axis=1)), 'tp')  5.73 us
    dot_general x1, matrix products, local(): lax.dot_general(cotangent, out_weight, (((1,), (1,)), ((), ())), preferre...  4.27 us
  transfers between devices with their start and end apart: 2, of which 2 were waited for; matrix products, arithmetic and copies ran while one was open for 19% of the time, Pallas kernels for 0%

profile of v1, /device:TPU:0, one launch (start us, length us, event | category | flops | bytes accessed | tf_op | source)
XLA Modules:
  0.0 203.8 jit_solution(18417188044386458879)
XLA Ops:
  7.2 0.0 copy-start
  7.2 0.0 all-reduce.5.cloned.1.call-start
  7.2 1.3 fusion.2
  8.6 0.7 convert_element_type.26
  9.3 8.3 %all-reduce.2 = (f32[512]{0:T(512)S(1)}, f32[512]{0:T(512)S(1)}) all-reduce(f32[512]{0:T(512)S(1)} %get-tuple-element.38, f32[512]{0:T(512)S(1)} %get-tuple-element.37), channel_id=1, replica_groups=mesh['sp'=8,'tp'=4] {'tp'}, use_global_device_ids=true, to_apply=%region_3.0 | all-reduce | flops 1024 | bytes 8192 | tf_op jit(solution)/shard_map/psum | solution.py:23
  17.6 0.0 copy-done
  17.6 4.3 %fusion.54 = (f32[512]{0:T(512)S(1)}, f32[512]{0:T(512)S(1)}, f32[512,504]{0,1:T(8,128)}) fusion(f32[512]{0:T(512)S(1)} %get-tuple-element.77, f32[512]{0:T(512)S(1)} %get-tuple-element.78, bf16[512,504]{0,1:T(8,128)(2,1)} %param.9, f32[504]{0:T(512)S(1)} %convert_element_type.26, bf16[512,2016]{0,1:T(8,128)(2,1)S(1)} %copy-done, bf16[504,2016]{1,0:T(8,128)(2,1)} %param.12), kind=kOutput, calls=%fused_computation.159 | convolution fusion | flops 1044577280 | bytes 5655008 | tf_op jit(solution)/shard_map/dot_general | solution.py:38
  21.9 5.7 %all-reduce.1 = (f32[512]{0:T(512)S(1)}, f32[512]{0:T(512)S(1)}) all-reduce(f32[512]{0:T(512)S(1)} %get-tuple-element.36, f32[512]{0:T(512)S(1)} %get-tuple-element.35), channel_id=1, replica_groups=mesh['sp'=8,'tp'=4] {'tp'}, use_global_device_ids=true, to_apply=%region_7.0 | all-reduce | flops 1024 | bytes 8192 | tf_op jit(solution)/shard_map/psum | solution.py:42
  27.6 0.0 copy-start.3
  27.6 1.7 fusion.17
  29.3 0.7 slice.249
  30.0 1.5 collective-permute-start
  31.5 0.0 copy-done.3
  31.5 3.4 %convolution_bitcast_fusion = f32[2016,504]{0,1:T(8,128)} fusion(bf16[512,2016]{0,1:T(8,128)(2,1)S(1)} %copy-done, bf16[512,504]{0,1:T(8,128)(2,1)S(1)} %copy-done.3, f32[504]{0:T(512)S(1)} %convert_element_type.26, f32[512]{0:T(512)S(1)} %get-tuple-element.78, f32[512]{0:T(512)S(1)} %get-tuple-element.77), kind=kOutput, calls=%fused_computation.29 | convolution fusion | flops 1042771968 | bytes 6650848 | tf_op jit(solution)/shard_map/dot_general | solution.py:33
  34.9 0.0 copy-start.4
  34.9 0.0 copy-start.5
  35.0 0.0 all-reduce.5.cloned.1.call-update
  35.0 0.7 copy-done.4
  35.8 0.0 copy-done.5
  35.8 0.6 dynamic-slice
  37.0 3.0 %collective-permute-done = f32[30,504]{0,1:T(8,128)S(1)} collective-permute-done((f32[30,504]{0,1:T(8,128)}, f32[30,504]{0,1:T(8,128)S(1)}, u32[]{:S(2)}, u32[]{:S(2)}) %collective-permute-start) | collective-permute-done | bytes 60512 | tf_op jit(solution)/shard_map/ppermute | solution.py:13
  40.0 0.0 copy-start.1
  40.0 0.0 copy-start.2
  40.0 17.6 %multiply_convert_fusion = (bf16[512,504]{0,1:T(8,128)(2,1)}, f32[512,504]{0,1:T(8,128)S(1)}) fusion(bf16[512,504]{0,1:T(8,128)(2,1)} %param.8, bf16[512,504]{0,1:T(8,128)(2,1)} %param.7, f32[512,504]{0,1:T(8,128)S(1)} %fusion.17, f32[504]{0:T(512)S(1)} %bitcast.111, f32[30,504]{0,1:T(8,128)S(1)} %collective-permute-done, f32[504]{0:T(512)S(1)} %bitcast.110, ...), kind=kLoop, calls=%fused_computation.142 | loop fusion | flops 26062848 | bytes 3735648 | tf_op jit(solution)/shard_map/convert_element_type | solution.py:59
  57.7 0.0 copy-done.1
  57.7 0.0 copy-done.2
  57.7 4.1 %multiply_reduce_fusion.4 = (f32[504]{0:T(512)S(1)}, f32[504]{0:T(512)S(1)}, f32[504]{0:T(512)S(1)}, f32[504]{0:T(512)S(1)}, f32[504]{0:T(512)S(1)}, /*index=5*/...) fusion(f32[30,504]{0,1:T(8,128)S(1)} %collective-permute-done, f32[512,504]{0,1:T(8,128)S(1)} %fusion.17, ...), kind=kLoop, calls=%fused_computation.115 | loop fusion | flops 7221816 | bytes 3687264 | tf_op jit(solution)/shard_map/reduce_sum | solution.py:56
  61.8 4.3 %multiply_reduce_fusion.1 = (f32[504]{0:T(512)S(1)}, f32[504]{0:T(512)S(1)}, f32[504]{0:T(512)S(1)}, f32[504]{0:T(512)S(1)}, f32[504]{0:T(512)S(1)}, /*index=5*/f32[504]{0:T(512)S(1)}, f32[504]{0:T(512)S(1)}, f32[504]{0:T(512)S(1)}) fusion(f32[30,504]{0,1:T(8,128)S(1)} %collective-permute-done, f32[512,504]{0,1:T(8,128)S(1)} %fusion.17, ...), kind=kLoop, calls=%fused_computation.112 | loop fusion | flops 7737408 | bytes 2140992 | tf_op jit(solution)/shard_map/reduce_sum | solution.py:56
  66.1 4.4 %multiply_reduce_fusion.2 = (f32[504]{0:T(512)S(1)}, f32[504]{0:T(512)S(1)}, f32[504]{0:T(512)S(1)}, f32[504]{0:T(512)S(1)}, f32[504]{0:T(512)S(1)}, /*index=5*/f32[504]{0:T(512)S(1)}, f32[504]{0:T(512)S(1)}, f32[504]{0:T(512)S(1)}) fusion(f32[30,504]{0,1:T(8,128)S(1)} %collective-permute-done, f32[512,504]{0,1:T(8,128)S(1)} %fusion.17, ...), kind=kLoop, calls=%fused_computation.113 | loop fusion | flops 7737408 | bytes 2140992 | tf_op jit(solution)/shard_map/reduce_sum | solution.py:56
  70.4 4.4 %multiply_reduce_fusion.3 = (f32[504]{0:T(512)S(1)}, f32[504]{0:T(512)S(1)}, f32[504]{0:T(512)S(1)}, f32[504]{0:T(512)S(1)}, f32[504]{0:T(512)S(1)}, /*index=5*/f32[504]{0:T(512)S(1)}, f32[504]{0:T(512)S(1)}, f32[504]{0:T(512)S(1)}) fusion(f32[30,504]{0,1:T(8,128)S(1)} %collective-permute-done, f32[512,504]{0,1:T(8,128)S(1)} %fusion.17, ...), kind=kLoop, calls=%fused_computation.114 | loop fusion | flops 7737408 | bytes 2140992 | tf_op jit(solution)/shard_map/reduce_sum | solution.py:56
  74.8 0.1 stack.127
  75.0 33.6 %all-gather.1 = f32[8,31,504]{2,1,0:T(8,128)S(1)} all-gather(f32[1,31,504]{2,1,0:T(8,128)S(1)} %bitcast.73), channel_id=2, replica_groups=mesh['sp'=8,'tp'=4] {'sp'}, dimensions={0}, use_global_device_ids=true | all-gather | bytes 562464 | tf_op jit(solution)/shard_map/all_gather | solution.py:57
  108.6 0.6 broadcast_multiply_fusion
  109.2 85.6 %all-reduce.5.cloned.1.call-done = f32[2016,504]{0,1:T(8,128)} async-done(((f32[2016,504]{0,1:T(8,128)}), f32[2016,504]{0,1:T(8,128)}) %all-reduce.5.cloned.1.call-update) | async-done | bytes 4064272
  194.9 2.1 %fusion.48 = f32[504,252]{1,0:T(8,128)} fusion(f32[2016,504]{0,1:T(8,128)} %all-reduce.5.cloned.1.call-done, u32[]{:T(128)S(6)} %multiply.5), kind=kLoop, calls=%fused_computation.148 | loop fusion | flops 127008 | bytes 1016068 | tf_op jit(solution)/shard_map/mul | solution.py:37
  (5 shorter events, 0.1 us)
Async XLA Ops:
  7.2 10.4 %copy-start = (bf16[512,2016]{0,1:T(8,128)(2,1)S(1)}, bf16[512,2016]{0,1:T(8,128)(2,1)}, u32[]{:S(2)}) copy-start(bf16[512,2016]{0,1:T(8,128)(2,1)} %param.13) | copy-start | bytes 6193156
  7.2 187.7 %all-reduce.5.cloned.1.call-start = ((), (), s32[]{:S(2)}) async-start(), calls=%async_computation | async-start | bytes 8257536
  27.6 3.9 %copy-start.3 = (bf16[512,504]{0,1:T(8,128)(2,1)S(1)}, bf16[512,504]{0,1:T(8,128)(2,1)}, u32[]{:S(2)}) copy-start(bf16[512,504]{0,1:T(8,128)(2,1)} %param.9) | copy-start | bytes 1548292
  30.0 10.0 %collective-permute-start = (f32[30,504]{0,1:T(8,128)}, f32[30,504]{0,1:T(8,128)S(1)}, u32[]{:S(2)}, u32[]{:S(2)}) collective-permute-start(f32[30,504]{0,1:T(8,128)} %slice.249), channel_id=1, source_target_pairs={{4,0},{8,4},{12,8},{16,12},{20,16},{24,20},{28,24},{5,1},{9,5},{13... | collective-permute-start | bytes 181448 | tf_op jit(solution)/shard_map/ppermute | solution.py:13
  34.9 0.8 copy-start.4
  34.9 0.8 copy-start.5
  40.0 17.7 %copy-start.1 = (bf16[512,504]{0,1:T(8,128)(2,1)S(1)}, bf16[512,504]{0,1:T(8,128)(2,1)}, u32[]{:S(2)}) copy-start(bf16[512,504]{0,1:T(8,128)(2,1)} %param.8) | copy-start | bytes 1548292
  40.0 17.7 %copy-start.2 = (bf16[512,504]{0,1:T(8,128)(2,1)S(1)}, bf16[512,504]{0,1:T(8,128)(2,1)}, u32[]{:S(2)}) copy-start(bf16[512,504]{0,1:T(8,128)(2,1)} %param.7) | copy-start | bytes 1548292
Sparse Core Ops, SparseCore 0:
  35.1 159.7 all-reduce.4
